TPU v7x, 512 devices: a whole 4x4x16 slice. The times are simulated.
512 devices in a mesh: sp: 64 (over z, y), tp: 8 (over x, core).
Axes of the slice: x: 4, y: 4, z: 16, core: 2. Of those that a mesh axis runs over, the one named last changes fastest.
Arguments:
- residual_signal: bfloat16 [16384, 2048], P('sp'), may hold values from -6 to 6
- reading_probe_preactivations: bfloat16 [16384, 1024], P('sp', 'tp'), may hold values from -6 to 6
- keep_switch_preactivations: bfloat16 [16384, 1024], P('sp', 'tp'), may hold values from -5.5 to 5.5
- written_entries: bfloat16 [16384, 1024], P('sp', 'tp'), may hold values from -6 to 6
- emission_switch_preactivations: bfloat16 [16384, 1024], P('sp', 'tp'), may hold values from -6 to 6
- additional_shrink_amount: float32 [16384, 1024], P('sp', 'tp'), may hold values from -0.7 to 0
- complement_of_floor: float32 [1024], P('tp'), may hold values from 6.1035156e-06 to 0.1
- per_group_rescaler: float32 [128], replicated, may hold values from 0.1 to 1.9
- emission_linear_map: bfloat16 [1024, 2048], P('tp'), may hold values from -0.1875 to 0.1875
- channel_layer_rescaler: float32 [2048], replicated, may hold values from 0.1 to 1.9
- expanding_linear_map: bfloat16 [2048, 8192], P('sp', 'tp'), may hold values from -0.125 to 0.125
- contracting_linear_map: bfloat16 [2048, 8192], P('sp', 'tp'), may hold values from -0.0625 to 0.0625
Outputs:
- layer_out: bfloat16 [16384, 2048], P('sp')
All inputs are finite; a program needn't handle non-finite values.
Results may differ from a plain program's by a relative error of at most 0.006.
Values may be sent and summed in bfloat16 or wider, within the bound.
A program may use at most 64 MiB of HBM per device.

v0:
```python
import jax
import jax.numpy as jnp
from jax import lax
from jax.sharding import Mesh
from jax.sharding import PartitionSpec as P

HEAD = 128
BLOCK = 64
SP = ("sp_0", "sp_1")
norm_eps = 1e-06
HIGH_ACCURACY = lax.Precision.HIGHEST


def filled_with(shard, identity):
    return jax.tree.map(
        lambda a, e: jnp.broadcast_to(jnp.asarray(e, a.dtype), a.shape), shard, identity
    )


def gathered_once(shard, axis):
    leaves = jax.tree.leaves(shard)
    turns = sorted(range(len(leaves)), key=lambda k: -leaves[k].size)
    width = (1, *leaves[turns[0]].shape)[-1]
    lines = [
        jnp.pad(leaves[k].reshape(-1), (0, -leaves[k].size % width)).reshape(-1, width)
        for k in turns
    ]
    both, at, found = (lax.all_gather(jnp.concatenate(lines), axis), 0, {})
    for k, line in zip(turns, lines):
        piece = both[:, at : at + len(line)].reshape(len(both), -1)
        found[k] = piece[:, : leaves[k].size].reshape(-1, *leaves[k].shape)
        at += len(line)
    numbers = iter(range(len(leaves)))
    return jax.tree.map(lambda _: found[next(numbers)], shard)


def entering(shard, axes, combine, identity):
    before = start = filled_with(shard, identity)
    total = shard
    for axis in reversed(axes):
        peers, index = (lax.axis_size(axis), lax.axis_index(axis))
        pieces = gathered_once(total, axis)
        inside, total = (start, start)
        for k in range(peers):
            passed = k < index
            total = combine(total, jax.tree.map(lambda part: part[k], pieces))
            inside = jax.tree.map(lambda new, old: jnp.where(passed, new, old), total, inside)
        before = combine(inside, before)
    return before


def laid_out(blocks, dim):
    lengths = list(blocks.shape[1:])
    lengths[dim] *= blocks.shape[0]
    return jnp.moveaxis(blocks, 0, dim).reshape(lengths)


def copy_for_each(shard, axis):
    peers = lax.axis_size(axis)
    return lax.all_to_all(
        jnp.broadcast_to(shard[None], (peers, *shard.shape)), axis, 0, 0, tiled=True
    )


def gathered_copies(shard, axis, dim):
    return laid_out(copy_for_each(shard, axis), dim)


def in_one_piece(arrays, axis, dim, along):
    widths = [a.shape[along] for a in arrays]
    both = jnp.concatenate(arrays, axis=along)
    whole = lax.all_gather(both, axis, axis=dim, tiled=True)
    return tuple(jnp.split(whole, [sum(widths[:k]) for k in range(1, len(widths))], axis=along))


def cut_along(shard, dim, peers):
    lengths = shard.shape
    blocks = shard.reshape(*lengths[:dim], peers, lengths[dim] // peers, *lengths[dim + 1 :])
    return jnp.moveaxis(blocks, dim, 0)


def sum_at_owner(shard, axis, dim):
    blocks = cut_along(shard, dim, lax.axis_size(axis))
    arrived = lax.all_to_all(blocks, axis, split_axis=0, concat_axis=0, tiled=True)
    return arrived.astype(jnp.float32).sum(axis=0)


def block_step(state_matrix, inputs):
    query_block_rows, key_blk, logs_blk, value_block_rows = inputs
    cumulative_decay = jnp.cumsum(logs_blk, axis=1)
    carried_state = jnp.einsum(
        "rlb,rbz->rlz",
        query_block_rows * jnp.exp(cumulative_decay),
        state_matrix,
        precision=HIGH_ACCURACY,
    )
    spread = cumulative_decay[:, :, None, :] - cumulative_decay[:, None, :, :]
    places = jnp.arange(BLOCK)
    lower = places[:, None] >= places[None, :]
    decay = jnp.exp(jnp.where(lower[None, :, :, None], spread, -jnp.inf))
    scores = jnp.einsum(
        "htk,hsk,htsk->hts", query_block_rows, key_blk, decay, precision=HIGH_ACCURACY
    )
    result = carried_state + jnp.einsum(
        "hts,hsv->htv", scores, value_block_rows, precision=HIGH_ACCURACY
    )
    final_state = cumulative_decay[:, -1:, :]
    decayed_key_rows = key_blk * jnp.exp(final_state - cumulative_decay)
    state_matrix = jnp.exp(final_state[:, 0, :])[..., None] * state_matrix + jnp.einsum(
        "aux,auf->axf", decayed_key_rows, value_block_rows, precision=HIGH_ACCURACY
    )
    return (state_matrix, result)


def combine_carry(earlier, later):
    return (earlier[0] * later[0], later[0][..., None] * earlier[1] + later[1])


def body(
    residual_signal,
    reading_probe_preactivations,
    keep_switch_preactivations,
    written_entries,
    emission_switch_preactivations,
    additional_shrink_amount,
    complement_of_floor,
    per_group_rescaler,
    emission_linear_map,
    channel_layer_rescaler,
    expanding_linear_map,
    contracting_linear_map,
):
    positions = reading_probe_preactivations.shape[0]
    channels = reading_probe_preactivations.shape[1]
    local_heads = channels // HEAD
    count = positions // BLOCK
    query_act = jax.nn.silu(reading_probe_preactivations.astype(jnp.float32))
    logarithmic_keep_fraction = (
        jnp.logaddexp(
            jnp.log1p(-complement_of_floor),
            jnp.log(complement_of_floor)
            + jax.nn.log_sigmoid(keep_switch_preactivations.astype(jnp.float32)),
        )
        + additional_shrink_amount
    )
    key_part = -jnp.expm1(logarithmic_keep_fraction)
    value_part = written_entries.astype(jnp.float32)

    def to_blocks(values):
        return values.reshape(count, BLOCK, local_heads, HEAD).transpose(0, 2, 1, 3)

    start = jnp.zeros((local_heads, HEAD, HEAD), jnp.float32)
    state_end, outputs = lax.scan(
        block_step,
        start,
        (
            to_blocks(query_act),
            to_blocks(key_part),
            to_blocks(logarithmic_keep_fraction),
            to_blocks(value_part),
        ),
    )
    within_block_output = outputs.transpose(0, 2, 1, 3).reshape(positions, local_heads, HEAD)
    running = jnp.cumsum(logarithmic_keep_fraction, axis=0)
    decay_total = jnp.exp(running[-1]).reshape(local_heads, HEAD)
    identity = (
        jnp.ones((local_heads, HEAD), jnp.float32),
        jnp.zeros((local_heads, HEAD, HEAD), jnp.float32),
    )
    prior_state = entering((decay_total, state_end), SP, combine_carry, identity)
    weighted_scores = (query_act * jnp.exp(running)).reshape(positions, local_heads, HEAD)
    recurrent_output = within_block_output + jnp.einsum(
        "pnm,nmx->pnx", weighted_scores, prior_state[1], precision=HIGH_ACCURACY
    )
    scaled = (
        recurrent_output
        * lax.rsqrt(
            jnp.mean(recurrent_output * recurrent_output, axis=-1, keepdims=True) + norm_eps
        )
        * per_group_rescaler
    )
    gated = scaled * jax.nn.silu(emission_switch_preactivations.astype(jnp.float32)).reshape(
        positions, local_heads, HEAD
    )
    mixed_heads = gated.reshape(positions, channels).astype(jnp.bfloat16)
    all_heads = gathered_copies(mixed_heads, "tp", 1)
    full_out = lax.all_gather(emission_linear_map, "tp", axis=0, tiled=True)
    projected = jnp.dot(all_heads, full_out, preferred_element_type=jnp.float32)
    after_mix = residual_signal.astype(jnp.float32) + projected
    normed = (
        after_mix
        * lax.rsqrt(jnp.mean(after_mix * after_mix, axis=-1, keepdims=True) + norm_eps)
        * channel_layer_rescaler
    ).astype(jnp.bfloat16)
    up_whole, down_whole = in_one_piece((expanding_linear_map, contracting_linear_map), SP, 0, 1)
    upward = jnp.dot(normed, up_whole, preferred_element_type=jnp.float32)
    hidden = jnp.square(jax.nn.relu(upward)).astype(jnp.bfloat16)
    share = positions // lax.axis_size("tp")
    downward = sum_at_owner(
        lax.dot_general(
            hidden, down_whole, (((1,), (1,)), ((), ())), preferred_element_type=jnp.float32
        ).astype(jnp.bfloat16),
        "tp",
        0,
    )
    own_start = lax.axis_index("tp") * share
    own_mix = lax.dynamic_slice_in_dim(after_mix, own_start, share, 0)
    finished = (own_mix + downward).astype(jnp.bfloat16)
    return gathered_copies(finished, "tp", 0)


def solution(mesh):
    finer = Mesh(mesh.devices.reshape(16, 4, mesh.shape["tp"]), ("sp_0", "sp_1", "tp"))
    return jax.shard_map(
        body,
        mesh=finer,
        in_specs=(
            P(SP, None),
            P(SP, "tp"),
            P(SP, "tp"),
            P(SP, "tp"),
            P(SP, "tp"),
            P(SP, "tp"),
            P("tp"),
            P(),
            P("tp", None),
            P(),
            P(SP, "tp"),
            P(SP, "tp"),
        ),
        out_specs=P(SP, None),
        check_vma=False,
    )
```

profile of v0, /device:TPU:1, one launch (start us, length us, event | category | flops | bytes accessed | tf_op | source)
XLA Modules:
  0.0 363.2 jit_solution(13176499211492240413)
XLA Ops:
  6.5 0.7 negate_log-plus-one_fusion
  7.2 1.1 exponential-minus-one_negate_fusion
  8.9 1.0 copy.41
  10.1 13.1 %while.13 = (s32[]{:T(128)}, f32[1,128,128]{2,1,0:T(8,128)S(1)}, f32[4,1,64,128]{3,2,1,0:T(8,128)S(1)}, f32[4,1,64,128]{3,2,1,0:T(8,128)S(1)}, f32[4,1,64,128]{3...) while((s32[]{:T(128)}, f32[1,128,128]{2,1,0:T(8,128)S(1)}, ...), condition=%wide.region_2.3_spmd.clone, body=%wide.region_0.2_spmd.clone.sunk | while | flops 34693120 | bytes 5108864 | solution.py:153
  10.2 0.6 select_exponential_fusion.2
  10.8 1.7 fusion.174
  13.0 0.3 fusion.172
  13.5 0.6 select_exponential_fusion.2
  14.1 1.7 fusion.174
  16.3 0.3 fusion.172
  16.7 0.6 select_exponential_fusion.2
  17.4 1.7 fusion.174
  19.5 0.3 fusion.172
  20.0 0.6 select_exponential_fusion.2
  20.6 1.7 fusion.174
  22.8 0.3 fusion.172
  23.2 10.7 %all-gather.2 = f32[4,129,128]{2,1,0:T(8,128)S(1)} all-gather(f32[1,129,128]{2,1,0:T(8,128)S(1)} %maximum_bitcast_fusion), channel_id=2, replica_groups=mesh['sp_0'=16,'sp_1'=4,'tp'=8] {'sp_1'}, dimensions={0}, use_global_device_ids=true | all-gather | bytes 330240 | tf_op jit(solution)/shard_map/all_gather | solution.py:28
  34.1 0.6 maximum_bitcast_fusion.1
  34.8 0.7 all-gather.8.cloned.1.call-update
  35.6 0.7 pad_maximum_fusion
  36.5 65.5 %all-gather.12.cloned.1.call-done = f32[16,129,128]{2,1,0:T(8,128)} async-done(((f32[1,129,128]{2,1,0:T(8,128)}), f32[16,129,128]{2,1,0:T(8,128)}) %all-gather.12.cloned.1.call-update) | async-done | bytes 1056784 | tf_op jit(solution)/shard_map/all_gather | solution.py:28
  102.1 0.8 slice_bitcast_fusion.16
  102.8 2.1 multiply_reduce_fusion.1
  105.1 24.3 %all_to_all.15 = bf16[8,256,128]{1,2,0:T(8,128)(2,1)S(1)} all-to-all(bf16[8,256,128]{1,2,0:T(8,128)(2,1)S(1)} %broadcast_in_dim.32), channel_id=1, replica_groups=mesh['sp_0'=16,'sp_1'=4,'tp'=8] {'tp'}, dimensions={0} | all-to-all | bytes 1048576 | tf_op jit(solution)/shard_map/all_to_all | solution.py:60
  129.4 22.2 %all-gather.8.cloned.1.call-done = bf16[1024,2048]{1,0:T(8,128)(2,1)} async-done(((bf16[128,2048]{1,0:T(8,128)(2,1)}), bf16[1024,2048]{1,0:T(8,128)(2,1)}) %all-gather.8.cloned.1.call-update) | async-done | bytes 4194320 | tf_op jit(solution)/shard_map/all_gather | solution.py:187
  151.7 3.9 %multiply_reduce_fusion = (f32[256]{0:T(256)S(1)}, f32[256,2048]{1,0:T(8,128)S(1)}) fusion(bf16[256,1024]{0,1:T(8,128)(2,1)S(1)} %bitcast.218, bf16[1024,2048]{1,0:T(8,128)(2,1)} %all-gather.8.cloned.1.call-done, bf16[256,2048]{1,0:T(8,128)(2,1)} %param.14), kind=kOutput, calls=%fused_computation.45 | convolution fusion | flops 1075838720 | bytes 7865344 | tf_op jit(solution)/shard_map/dot_general | solution.py:188
  155.5 147.1 %all-gather.10.cloned.1.call-done = bf16[2048,2048]{1,0:T(8,128)(2,1)} async-done(((bf16[32,2048]{1,0:T(8,128)(2,1)}), bf16[2048,2048]{1,0:T(8,128)(2,1)}) %all-gather.10.cloned.1.call-update) | async-done | bytes 8388624 | tf_op jit(solution)/shard_map/all_gather | solution.py:72
  302.7 6.8 %fusion.32 = bf16[256,2048]{1,0:T(8,128)(2,1)} fusion(bf16[2048,2048]{1,0:T(8,128)(2,1)} %all-gather.10.cloned.1.call-done, f32[256,2048]{1,0:T(8,128)S(1)} %get-tuple-element.142, f32[2048]{0:T(1024)S(1)} %copy-done.5, f32[256]{0:T(256)S(1)} %add_rsqrt_fusion), kind=kOutput, calls=%fused_computation.42 | convolution fusion | flops 2150367232 | bytes 11543552 | tf_op jit(solution)/shard_map/dot_general | solution.py:200
  309.5 12.7 %all-to-all-start.1 = ((bf16[8,32,2048]{2,1,0:T(8,128)(2,1)}), bf16[8,32,2048]{2,1,0:T(8,128)(2,1)S(1)}, u32[]{:S(2)}, u32[]{:S(2)}) async-start(bf16[8,32,2048]{2,1,0:T(8,128)(2,1)} %bitcast.223), calls=%async_computation.1 | async-start | bytes 2097152 | tf_op jit(solution)/shard_map/all_to_all | solution.py:84
  322.2 15.0 %all-to-all-done.1 = bf16[8,32,2048]{2,1,0:T(8,128)(2,1)S(1)} async-done(((bf16[8,32,2048]{2,1,0:T(8,128)(2,1)}), bf16[8,32,2048]{2,1,0:T(8,128)(2,1)S(1)}, u32[]{:S(2)}, u32[]{:S(2)}) %all-to-all-start.1) | async-done | bytes 1048608 | tf_op jit(solution)/shard_map/all_to_all | solution.py:84
  337.4 18.3 %all_to_all.16 = bf16[8,32,2048]{2,1,0:T(8,128)(2,1)S(1)} all-to-all(bf16[8,32,2048]{2,1,0:T(8,128)(2,1)S(1)} %broadcast_in_dim.33), channel_id=1, replica_groups=mesh['sp_0'=16,'sp_1'=4,'tp'=8] {'tp'}, dimensions={0} | all-to-all | bytes 2097152 | tf_op jit(solution)/shard_map/all_to_all | solution.py:60
  355.7 1.0 copy.80
  (78 shorter events, 3.8 us)
Async XLA Ops:
  6.5 3.5 copy-start
  6.5 95.5 %all-gather.12.cloned.1.call-start = ((), (), s32[]{:S(2)}) async-start(), calls=%async_computation.5 | async-start | bytes 1183744 | tf_op jit(solution)/shard_map/all_gather | solution.py:28
  10.0 25.5 %copy-start.2 = (bf16[32,1024]{1,0:T(8,128)(2,1)S(1)}, bf16[32,1024]{1,0:T(8,128)(2,1)}, u32[]{:S(2)}) copy-start(bf16[32,1024]{1,0:T(8,128)(2,1)} %param.25) | copy-start | bytes 196612
  10.1 25.5 %copy-start.3 = (bf16[32,1024]{1,0:T(8,128)(2,1)S(1)}, bf16[32,1024]{1,0:T(8,128)(2,1)}, u32[]{:S(2)}) copy-start(bf16[32,1024]{1,0:T(8,128)(2,1)} %param.24) | copy-start | bytes 196612
  23.1 13.3 %copy-start.1 = (bf16[256,128]{1,0:T(8,128)(2,1)S(1)}, bf16[256,128]{1,0:T(8,128)(2,1)}, u32[]{:S(2)}) copy-start(bf16[256,128]{1,0:T(8,128)(2,1)} %param.18) | copy-start | bytes 196612
  34.7 70.2 %copy-start.4 = (f32[128]{0:T(128)S(1)}, f32[128]{0:T(128)}, u32[]{:S(2)}) copy-start(f32[128]{0:T(128)} %param.21) | copy-start | bytes 1540
  34.7 116.9 %all-gather.8.cloned.1.call-start = ((), (), s32[]{:S(2)}) async-start(), calls=%async_computation.3 | async-start | bytes 4718592 | tf_op jit(solution)/shard_map/all_gather | solution.py:187
  35.5 267.2 %all-gather.10.cloned.1.call-start = ((), (), s32[]{:S(2)}) async-start(), calls=%async_computation.4 | async-start | bytes 8519680 | tf_op jit(solution)/shard_map/all_gather | solution.py:72
  151.7 151.0 %copy-start.5 = (f32[2048]{0:T(1024)S(1)}, f32[2048]{0:T(1024)}, u32[]{:S(2)}) copy-start(f32[2048]{0:T(1024)} %param.23) | copy-start | bytes 24580
  309.5 27.6 %all-to-all-start.1 = ((bf16[8,32,2048]{2,1,0:T(8,128)(2,1)}), bf16[8,32,2048]{2,1,0:T(8,128)(2,1)S(1)}, u32[]{:S(2)}, u32[]{:S(2)}) async-start(bf16[8,32,2048]{2,1,0:T(8,128)(2,1)} %bitcast.223), calls=%async_computation.1 | async-start | bytes 2097152 | tf_op jit(solution)/shard_map/all_to_all | solution.py:84
Sparse Core Ops, SparseCore 0:
  34.8 67.1 all-gather.11
  104.2 47.3 all-gather.7
  154.6 148.0 all-gather.9
where the time goes:
time: 364 us; the launch traced here: 363 us
  waiting for transfers between devices  251 us (69%)
  blocking collectives  53.4 us (15%)
  matrix products  15.7 us (4%)
  other arithmetic  14.3 us (4%)
  between operations  13.4 us (4%)
  starting transfers between devices  12.8 us (4%)
    all_gather x1, waiting for transfers between devices, in_one_piece(): whole = lax.all_gather(both, axis, axis=dim, tiled=True)  147 us
    all_gather x1, waiting for transfers between devices, gathered_once(): both, at, found = (lax.all_gather(jnp.concatenate(lines), axis), 0, {})  65.5 us
    all_to_all x2, blocking collectives, copy_for_each(): lax.all_to_all(jnp.broadcast_to(shard[None], (peers, *shard.shape)), axis...  42.6 us
    all_gather x1, waiting for transfers between devices, body(): full_out = lax.all_gather(emission_linear_map, 'tp', axis=0, tiled=True)  22.2 us
    all_to_all x1, waiting for transfers between devices, sum_at_owner(): lax.all_to_all(blocks, axis, split_axis=0, concat_axis=0, tiled=True)  15 us
    all_to_all x1, starting transfers between devices, sum_at_owner(): lax.all_to_all(blocks, axis, split_axis=0, concat_axis=0, tiled=True)  12.7 us
    all_gather x1, blocking collectives, gathered_once(): both, at, found = (lax.all_gather(jnp.concatenate(lines), axis), 0, {})  10.7 us
  transfers between devices with their start and end apart: 4, of which 4 were waited for; matrix products, arithmetic and copies ran while one was open for 2% of the time, Pallas kernels for 0%

commit v1 on v0

--- a/solution.py
+++ b/solution.py
@@ -9,6 +9,11 @@
 SP = ("sp_0", "sp_1")
 norm_eps = 1e-06
 HIGH_ACCURACY = lax.Precision.HIGHEST
+
+
+def tiled_gather(x, axis, dim):
+    copies = jnp.concatenate([x] * lax.axis_size(axis), axis=dim)
+    return lax.all_to_all(copies, axis, dim, dim, tiled=True)
 
 
 def filled_with(shard, identity):
@@ -184,7 +189,7 @@
     )
     mixed_heads = gated.reshape(positions, channels).astype(jnp.bfloat16)
     all_heads = gathered_copies(mixed_heads, "tp", 1)
-    full_out = lax.all_gather(emission_linear_map, "tp", axis=0, tiled=True)
+    full_out = tiled_gather(emission_linear_map, "tp", 0)
     projected = jnp.dot(all_heads, full_out, preferred_element_type=jnp.float32)
     after_mix = residual_signal.astype(jnp.float32) + projected
     normed = (

time: 364 us -> 323 us (0.89)
  waiting for transfers between devices: 251 us -> 159 us
  blocking collectives: 53.4 us -> 82.4 us
  starting transfers between devices: 12.8 us -> 27.9 us
  local copies, waits for them, and re-layouts: 2.83 us -> 10.5 us
    all_gather x1, waiting for transfers between devices: 147 us -> 75.3 us  [in_one_piece(): whole = lax.all_gather(both, axis, axis=dim, tiled=True)]
    all_to_all x0 -> x1, blocking collectives: none -> 53.3 us  [tiled_gather(): return lax.all_to_all(copies, axis, dim, dim, tiled=True)]
    all_to_all x2 -> x1, blocking collectives: 42.6 us -> 18.3 us  [copy_for_each(): lax.all_to_all(jnp.broadcast_to(shard[None], (peers, *shard.shape)), axis...]
    all_gather x1 -> x0, waiting for transfers between devices: 22.2 us -> none  [body(): full_out = lax.all_gather(emission_linear_map, 'tp', axis=0, tiled=True)]
    all_to_all x0 -> x1, starting transfers between devices: none -> 15.2 us  [copy_for_each(): lax.all_to_all(jnp.broadcast_to(shard[None], (peers, *shard.shape)), axis...]
    all_to_all x0 -> x1, waiting for transfers between devices: none -> 7.7 us  [copy_for_each(): lax.all_to_all(jnp.broadcast_to(shard[None], (peers, *shard.shape)), axis...]
    unnamed x17 -> x26, local copies, waits for them, and re-layouts: 2.1 us -> 7.96 us
    all_gather x1, waiting for transfers between devices: 65.5 us -> 61.3 us  [gathered_once(): both, at, found = (lax.all_gather(jnp.concatenate(lines), axis), 0, {})]
  transfers between devices with their start and end apart: 4 -> 4, of which waited for: 4 -> 4; matrix products, arithmetic and copies ran while one was open for 2% -> 4% of each run, Pallas kernels for 0% -> 0%
where the time goes in v1:
time: 323 us; the launch traced here: 322 us
  waiting for transfers between devices  159 us (49%)
  blocking collectives  82.4 us (26%)
  starting transfers between devices  27.9 us (9%)
  other arithmetic  15.1 us (5%)
  between operations  13.7 us (4%)
  matrix products  13.3 us (4%)
  local copies, waits for them, and re-layouts  10.5 us (3%)
    all_gather x1, waiting for transfers between devices, in_one_piece(): whole = lax.all_gather(both, axis, axis=dim, tiled=True)  75.3 us
    all_gather x1, waiting for transfers between devices, gathered_once(): both, at, found = (lax.all_gather(jnp.concatenate(lines), axis), 0, {})  61.3 us
    all_to_all x1, blocking collectives, tiled_gather(): return lax.all_to_all(copies, axis, dim, dim, tiled=True)  53.3 us
    all_to_all x1, blocking collectives, copy_for_each(): lax.all_to_all(jnp.broadcast_to(shard[None], (peers, *shard.shape)), axis...  18.3 us
    all_to_all x1, starting transfers between devices, copy_for_each(): lax.all_to_all(jnp.broadcast_to(shard[None], (peers, *shard.shape)), axis...  15.2 us
    all_to_all x1, waiting for transfers between devices, sum_at_owner(): lax.all_to_all(blocks, axis, split_axis=0, concat_axis=0, tiled=True)  15 us
    all_to_all x1, starting transfers between devices, sum_at_owner(): lax.all_to_all(blocks, axis, split_axis=0, concat_axis=0, tiled=True)  12.7 us
    all_gather x1, blocking collectives, gathered_once(): both, at, found = (lax.all_gather(jnp.concatenate(lines), axis), 0, {})  10.7 us
  transfers between devices with their start and end apart: 4, of which 4 were waited for; matrix products, arithmetic and copies ran while one was open for 4% of the time, Pallas kernels for 0%

profile of v1, /device:TPU:1, one launch (start us, length us, event | category | flops | bytes accessed | tf_op | source)
XLA Modules:
  0.0 322.4 jit_solution(15501872382240275079)
XLA Ops:
  7.2 1.1 exponential-minus-one_negate_fusion
  8.8 1.0 copy.43
  10.0 0.9 convert.1
  10.9 13.1 %while.13 = (s32[]{:T(128)}, f32[1,128,128]{2,1,0:T(8,128)S(1)}, f32[4,1,64,128]{3,2,1,0:T(8,128)S(1)}, f32[4,1,64,128]{3,2,1,0:T(8,128)S(1)}, f32[4,1,64,128]{3...) while((s32[]{:T(128)}, f32[1,128,128]{2,1,0:T(8,128)S(1)}, ...), condition=%wide.region_2.3_spmd.clone, body=%wide.region_0.2_spmd.clone.sunk | while | flops 34693120 | bytes 5108864 | solution.py:158
  11.7 1.7 fusion.175
  14.9 1.7 fusion.175
  18.2 1.7 fusion.175
  21.5 1.7 fusion.175
  24.0 10.7 %all-gather.2 = f32[4,129,128]{2,1,0:T(8,128)S(1)} all-gather(f32[1,129,128]{2,1,0:T(8,128)S(1)} %maximum_bitcast_fusion), channel_id=2, replica_groups=mesh['sp_0'=16,'sp_1'=4,'tp'=8] {'sp_1'}, dimensions={0}, use_global_device_ids=true | all-gather | bytes 330240 | tf_op jit(solution)/shard_map/all_gather | solution.py:33
  35.6 0.7 pad_maximum_fusion
  36.6 0.9 constant_dynamic-update-slice_fusion.7
  37.4 0.9 constant_dynamic-update-slice_fusion.6
  38.3 0.8 constant_dynamic-update-slice_fusion.5
  39.1 0.8 constant_dynamic-update-slice_fusion.4
  39.9 0.9 constant_dynamic-update-slice_fusion.3
  40.8 0.8 constant_dynamic-update-slice_fusion.2
  41.6 61.3 %all-gather.9.cloned.1.call-done = f32[16,129,128]{2,1,0:T(8,128)} async-done(((f32[1,129,128]{2,1,0:T(8,128)}), f32[16,129,128]{2,1,0:T(8,128)}) %all-gather.9.cloned.1.call-update) | async-done | bytes 1056784 | tf_op jit(solution)/shard_map/all_gather | solution.py:33
  102.9 0.8 slice_bitcast_fusion.16
  103.6 2.1 multiply_reduce_fusion.1
  106.0 0.9 broadcast_in_dim.32
  106.8 15.2 %all-to-all-start = ((bf16[8,256,128]{2,1,0:T(8,128)(2,1)}), bf16[8,256,128]{2,1,0:T(8,128)(2,1)S(1)}, u32[]{:S(2)}, u32[]{:S(2)}) async-start(bf16[8,256,128]{2,1,0:T(8,128)(2,1)} %broadcast_in_dim.32), calls=%async_computation | async-start | bytes 1048576 | tf_op jit(solution)/shard_map/all_to_all | solution.py:65
  122.0 0.8 constant_dynamic-update-slice_fusion.1
  122.8 0.8 constant_dynamic-update-slice_fusion
  123.7 7.7 %all-to-all-done = bf16[8,256,128]{2,1,0:T(8,128)(2,1)S(1)} async-done(((bf16[8,256,128]{2,1,0:T(8,128)(2,1)}), bf16[8,256,128]{2,1,0:T(8,128)(2,1)S(1)}, u32[]{:S(2)}, u32[]{:S(2)}) %all-to-all-start) | async-done | bytes 524320 | tf_op jit(solution)/shard_map/all_to_all | solution.py:65
  131.4 53.3 %all_to_all.24 = bf16[8,128,2048]{2,1,0:T(8,128)(2,1)S(1)} all-to-all(bf16[8,128,2048]{2,1,0:T(8,128)(2,1)} %bitcast.42), channel_id=1, replica_groups=mesh['sp_0'=16,'sp_1'=4,'tp'=8] {'tp'}, dimensions={0} | all-to-all | bytes 8388608 | tf_op jit(solution)/shard_map/all_to_all | solution.py:16
  184.7 1.5 multiply_reduce_fusion
  186.2 75.3 %all-gather.7.cloned.1.call-done = bf16[2048,2048]{1,0:T(8,128)(2,1)} async-done(((bf16[32,2048]{1,0:T(8,128)(2,1)}), bf16[2048,2048]{1,0:T(8,128)(2,1)}) %all-gather.7.cloned.1.call-update) | async-done | bytes 8388624 | tf_op jit(solution)/shard_map/all_gather | solution.py:77
  261.5 6.8 %fusion.33 = bf16[256,2048]{1,0:T(8,128)(2,1)} fusion(bf16[2048,2048]{1,0:T(8,128)(2,1)} %all-gather.7.cloned.1.call-done, f32[256,2048]{1,0:T(8,128)S(1)} %get-tuple-element.142, f32[2048]{0:T(1024)S(1)} %copy-done.6, f32[256]{0:T(256)S(1)} %add_rsqrt_fusion), kind=kOutput, calls=%fused_computation.43 | convolution fusion | flops 2150367232 | bytes 11543552 | tf_op jit(solution)/shard_map/dot_general | solution.py:205
  268.3 12.7 %all-to-all-start.2 = ((bf16[8,32,2048]{2,1,0:T(8,128)(2,1)}), bf16[8,32,2048]{2,1,0:T(8,128)(2,1)S(1)}, u32[]{:S(2)}, u32[]{:S(2)}) async-start(bf16[8,32,2048]{2,1,0:T(8,128)(2,1)} %bitcast.44), calls=%async_computation.2 | async-start | bytes 2097152 | tf_op jit(solution)/shard_map/all_to_all | solution.py:89
  281.0 15.0 %all-to-all-done.2 = bf16[8,32,2048]{2,1,0:T(8,128)(2,1)S(1)} async-done(((bf16[8,32,2048]{2,1,0:T(8,128)(2,1)}), bf16[8,32,2048]{2,1,0:T(8,128)(2,1)S(1)}, u32[]{:S(2)}, u32[]{:S(2)}) %all-to-all-start.2) | async-done | bytes 1048608 | tf_op jit(solution)/shard_map/all_to_all | solution.py:89
  296.3 18.3 %all_to_all.25 = bf16[8,32,2048]{2,1,0:T(8,128)(2,1)S(1)} all-to-all(bf16[8,32,2048]{2,1,0:T(8,128)(2,1)S(1)} %broadcast_in_dim.33), channel_id=1, replica_groups=mesh['sp_0'=16,'sp_1'=4,'tp'=8] {'tp'}, dimensions={0} | all-to-all | bytes 2097152 | tf_op jit(solution)/shard_map/all_to_all | solution.py:65
  314.6 1.0 copy.90
  (88 shorter events, 8.8 us)
Async XLA Ops:
  6.5 96.3 %all-gather.9.cloned.1.call-start = ((), (), s32[]{:S(2)}) async-start(), calls=%async_computation.5 | async-start | bytes 1183744 | tf_op jit(solution)/shard_map/all_gather | solution.py:33
  10.8 24.7 %copy-start.2 = (bf16[32,1024]{1,0:T(8,128)(2,1)S(1)}, bf16[32,1024]{1,0:T(8,128)(2,1)}, u32[]{:S(2)}) copy-start(bf16[32,1024]{1,0:T(8,128)(2,1)} %param.25) | copy-start | bytes 196612
  10.8 24.7 %copy-start.3 = (bf16[32,1024]{1,0:T(8,128)(2,1)S(1)}, bf16[32,1024]{1,0:T(8,128)(2,1)}, u32[]{:S(2)}) copy-start(bf16[32,1024]{1,0:T(8,128)(2,1)} %param.24) | copy-start | bytes 196612
  10.9 25.6 %copy-start.1 = (bf16[256,128]{1,0:T(8,128)(2,1)S(1)}, bf16[256,128]{1,0:T(8,128)(2,1)}, u32[]{:S(2)}) copy-start(bf16[256,128]{1,0:T(8,128)(2,1)} %param.18) | copy-start | bytes 196612
  10.9 25.7 %copy-start = (bf16[128,2048]{1,0:T(8,128)(2,1)S(1)}, bf16[128,2048]{1,0:T(8,128)(2,1)}, u32[]{:S(2)}) copy-start(bf16[128,2048]{1,0:T(8,128)(2,1)} %param.22) | copy-start | bytes 1572868
  35.5 226.0 %all-gather.7.cloned.1.call-start = ((), (), s32[]{:S(2)}) async-start(), calls=%async_computation.4 | async-start | bytes 8519680 | tf_op jit(solution)/shard_map/all_gather | solution.py:77
  37.4 68.3 %copy-start.4 = (f32[128]{0:T(128)S(1)}, f32[128]{0:T(128)}, u32[]{:S(2)}) copy-start(f32[128]{0:T(128)} %param.21) | copy-start | bytes 1540
  106.8 24.5 %all-to-all-start = ((bf16[8,256,128]{2,1,0:T(8,128)(2,1)}), bf16[8,256,128]{2,1,0:T(8,128)(2,1)S(1)}, u32[]{:S(2)}, u32[]{:S(2)}) async-start(bf16[8,256,128]{2,1,0:T(8,128)(2,1)} %broadcast_in_dim.32), calls=%async_computation | async-start | bytes 1048576 | tf_op jit(solution)/shard_map/all_to_all | solution.py:65
  131.4 53.3 %copy-start.5 = (bf16[256,2048]{1,0:T(8,128)(2,1)S(1)}, bf16[256,2048]{1,0:T(8,128)(2,1)}, u32[]{:S(2)}) copy-start(bf16[256,2048]{1,0:T(8,128)(2,1)} %param.14) | copy-start | bytes 3145732
  184.7 76.7 %copy-start.6 = (f32[2048]{0:T(1024)S(1)}, f32[2048]{0:T(1024)}, u32[]{:S(2)}) copy-start(f32[2048]{0:T(1024)} %param.23) | copy-start | bytes 24580
  268.3 27.6 %all-to-all-start.2 = ((bf16[8,32,2048]{2,1,0:T(8,128)(2,1)}), bf16[8,32,2048]{2,1,0:T(8,128)(2,1)S(1)}, u32[]{:S(2)}, u32[]{:S(2)}) async-start(bf16[8,32,2048]{2,1,0:T(8,128)(2,1)} %bitcast.44), calls=%async_computation.2 | async-start | bytes 2097152 | tf_op jit(solution)/shard_map/all_to_all | solution.py:89
Sparse Core Ops, SparseCore 0:
  35.6 67.1 all-gather.8
  105.8 155.6 all-gather.6
